TPU v7x, 32 devices: a whole 2x2x4 slice. The times are simulated.
32 devices in a mesh: sp: 4 (over z), tp: 4 (over y, x), dp: 2 (over core).
Axes of the slice: x: 2, y: 2, z: 4, core: 2. Of those that a mesh axis runs over, the one named last changes fastest.
Arguments:
- latent_tokens: bfloat16 [4096, 2048], P(('dp', 'sp', 'tp')), parts along dimension 0, may hold values from -6 to 6
- condition: bfloat16 [4096], P(('dp', 'sp')), parts along dimension 0, may hold values from -6 to 6
- shift_weight: bfloat16 [2048, 2048], P('sp', 'tp'), may hold values from -0.125 to 0.125
- scale_weight: bfloat16 [2048, 2048], P('sp', 'tp'), may hold values from -0.125 to 0.125
- gate_weight: bfloat16 [2048, 2048], P('sp', 'tp'), may hold values from -0.125 to 0.125
- norm_gain: float32 [2048], replicated, may hold values from 0.1 to 1.9
- query_down: bfloat16 [2048, 512], replicated, may hold values from -0.125 to 0.125
- query_gain: float32 [512], replicated, may hold values from 0.1 to 1.9
- kv_down: bfloat16 [2048, 256], replicated, may hold values from -0.125 to 0.125
- kv_gain: float32 [256], replicated, may hold values from 0.1 to 1.9
- rope_down: bfloat16 [2048, 32], replicated, may hold values from -0.125 to 0.125
- query_up: bfloat16 [512, 1536], P(None, 'tp'), may hold values from -0.25 to 0.25
- key_up: bfloat16 [256, 1024], P(None, 'tp'), may hold values from -0.375 to 0.375
- value_up: bfloat16 [256, 1024], P(None, 'tp'), may hold values from -0.375 to 0.375
- query_norm_gain: float32 [96], replicated, may hold values from 0.47 to 16
- key_norm_gain: float32 [96], replicated, may hold values from 0.47 to 16
- out_weight: bfloat16 [1024, 2048], P('tp'), may hold values from -0.1875 to 0.1875
- context_latent: bfloat16 [2048, 256], P(('dp', 'sp')), parts along dimension 0, may hold values from -6 to 6
- context_rope: bfloat16 [2048, 32], P(('dp', 'sp')), parts along dimension 0, may hold values from -6 to 6
- context_lift: float32 [16], P('tp'), may hold values from 0 to 2
Outputs:
- output: bfloat16 [4096, 2048], P(('dp', 'sp', 'tp')), parts along dimension 0
There are 2 independent parts, one for each index of `dp`. A program takes and returns all parts, laid end to end along the dimension named above; an argument that names none is the same for every part. Nothing has to cross between parts.
All inputs are finite; a program needn't handle non-finite values.
Results may differ from a plain program's by a relative error of at most 0.015.
The roundings to bfloat16 on the way count: a program that leaves them out, or rounds other values in their place, can miss the bound.
Values may be sent and summed in bfloat16 or wider, within the bound.
No kernel may reach another device: no remote copies, remote signals or barrier semaphores. Data moves between devices by JAX's collectives and lax.ppermute only.
A program may use at most 128 MiB of HBM per device.

v0:
```python
import jax
import jax.numpy as jnp
from jax import lax
from jax.sharding import PartitionSpec as P

NOPE_DIM = 64
ROPE_DIM = 32
VALUE_DIM = 64
QK_DIM = 96
GRID_W = 64


EPS = 1e-06
THETA = 10000.0


def rms_scaled(values, gain_vector):
    mean_square = jnp.mean(values * values, axis=-1, keepdims=True)
    return values * lax.rsqrt(mean_square + EPS) * gain_vector


def rotate(rope_part, positions):
    row_count = rope_part.shape[0]
    freq_count = ROPE_DIM // 4
    inverse = THETA ** (-4.0 * jnp.arange(freq_count, dtype=jnp.float32) / ROPE_DIM)
    grid_row = (positions // GRID_W).astype(jnp.float32)
    grid_col = (positions % GRID_W).astype(jnp.float32)
    angles = jnp.stack([grid_row[:, None] * inverse, grid_col[:, None] * inverse], axis=1)
    cosine_table = jnp.cos(angles)[:, None]
    sine_table = jnp.sin(angles)[:, None]
    split_rows = rope_part.reshape(row_count, rope_part.shape[1], 2, 2, freq_count)
    first_half = split_rows[:, :, :, 0]
    second_half = split_rows[:, :, :, 1]
    turned = jnp.stack(
        [
            first_half * cosine_table - second_half * sine_table,
            second_half * cosine_table + first_half * sine_table,
        ],
        axis=3,
    )
    return turned.reshape(rope_part.shape)


def build_keys(
    latent_rows, rope_rows, first_index, shard_rows, group_rows, key_up, value_up, key_norm_gain
):
    row_count = latent_rows.shape[0]
    head_count = key_up.shape[1] // NOPE_DIM
    nope_part = jnp.dot(latent_rows, key_up, preferred_element_type=jnp.float32).reshape(
        row_count, head_count, NOPE_DIM
    )
    value_rows = jnp.dot(latent_rows, value_up, preferred_element_type=jnp.float32).astype(
        jnp.bfloat16
    )
    shared = jnp.broadcast_to(
        rope_rows.astype(jnp.float32)[:, None, :], (row_count, head_count, ROPE_DIM)
    )
    normal_keys = rms_scaled(jnp.concatenate([nope_part, shared], axis=-1), key_norm_gain)
    row_index = first_index + jnp.arange(row_count, dtype=jnp.int32)
    within = row_index % shard_rows
    is_latent = within < group_rows
    positions = row_index // shard_rows * group_rows + within
    turned = rotate(normal_keys[..., NOPE_DIM:], positions)
    rope_part = jnp.where(is_latent[:, None, None], turned, normal_keys[..., NOPE_DIM:])
    key_rows = jnp.concatenate([normal_keys[..., :NOPE_DIM], rope_part], axis=-1).astype(
        jnp.bfloat16
    )
    return (key_rows.reshape(row_count, head_count * QK_DIM), value_rows)


def key_offset(first_index, row_count, shard_rows, group_rows, context_lift):
    row_index = first_index + jnp.arange(row_count, dtype=jnp.int32)
    is_context = row_index % shard_rows >= group_rows
    return jnp.where(is_context[None, :], context_lift[:, None], jnp.zeros((), jnp.float32))


def attend_block(carried, queries, key_rows, value_rows, offset):
    running_max, weight_sum, accumulated = carried
    row_count = key_rows.shape[0]
    head_count = queries.shape[1]
    key_heads = key_rows.reshape(row_count, head_count, QK_DIM)
    value_heads = value_rows.reshape(row_count, head_count, VALUE_DIM)
    scores = jnp.einsum(
        "qhd,khd->hqk", queries, key_heads, preferred_element_type=jnp.float32
    ) * QK_DIM ** (-0.5)
    scores = scores + offset[:, None, :]
    new_max = jnp.maximum(running_max, jnp.max(scores, axis=-1))
    factor = jnp.exp(running_max - new_max)
    weights = jnp.exp(scores - new_max[..., None])
    weight_sum = weight_sum * factor + jnp.sum(weights, axis=-1)
    product = jnp.einsum(
        "hqk,khd->qhd",
        weights.astype(jnp.bfloat16),
        value_heads,
        preferred_element_type=jnp.float32,
    )
    accumulated = accumulated * factor.T[:, :, None] + product
    return (new_max, weight_sum, accumulated)


def fold_blocks(carried, pieces, shard_rows, block_step):
    block_count = pieces[0].shape[0] // shard_rows
    blocked = tuple(
        (
            piece_rows.reshape((block_count, shard_rows) + piece_rows.shape[1:])
            for piece_rows in pieces
        )
    )
    starts = shard_rows * jnp.arange(block_count, dtype=jnp.int32)

    def one_block(state_now, inputs):
        return (block_step(state_now, inputs[:-1], inputs[-1]), None)

    final_state, ignored = lax.scan(one_block, carried, blocked + (starts,))
    return final_state


def local(
    latent_tokens,
    condition,
    shift_weight,
    scale_weight,
    gate_weight,
    norm_gain,
    query_down,
    query_gain,
    kv_down,
    kv_gain,
    rope_down,
    query_up,
    key_up,
    value_up,
    query_norm_gain,
    key_norm_gain,
    out_weight,
    context_latent,
    context_rope,
    context_lift,
):
    activated = jax.nn.silu(condition.astype(jnp.float32)).astype(jnp.bfloat16)[None]
    shift_term = jnp.dot(activated, shift_weight, preferred_element_type=jnp.float32)[0]
    scale_term = jnp.dot(activated, scale_weight, preferred_element_type=jnp.float32)[0]
    gate_term = jnp.dot(activated, gate_weight, preferred_element_type=jnp.float32)[0]
    shift_sum, scale_sum, gate_sum = lax.psum((shift_term, scale_term, gate_term), "sp")
    mod_shift, mod_scale, mod_gate = (
        lax.all_gather(shift_sum, "tp", axis=0, tiled=True),
        lax.all_gather(scale_sum, "tp", axis=0, tiled=True),
        lax.all_gather(gate_sum, "tp", axis=0, tiled=True),
    )
    token_values = latent_tokens.astype(jnp.float32)
    normed = (rms_scaled(token_values, norm_gain) * (1.0 + mod_scale) + mod_shift).astype(
        jnp.bfloat16
    )
    query_latent = rms_scaled(
        jnp.dot(normed, query_down, preferred_element_type=jnp.float32), query_gain
    ).astype(jnp.bfloat16)
    key_latent = rms_scaled(
        jnp.dot(normed, kv_down, preferred_element_type=jnp.float32), kv_gain
    ).astype(jnp.bfloat16)
    rope_key = jnp.dot(normed, rope_down, preferred_element_type=jnp.float32).astype(jnp.bfloat16)
    query_group, latent_group, rope_group = (
        lax.all_gather(query_latent, "tp", axis=0, tiled=True),
        lax.all_gather(key_latent, "tp", axis=0, tiled=True),
        lax.all_gather(rope_key, "tp", axis=0, tiled=True),
    )
    group_rows = query_group.shape[0]
    head_count = query_up.shape[1] // QK_DIM
    positions = lax.axis_index("sp") * group_rows + jnp.arange(group_rows, dtype=jnp.int32)
    query_heads = rms_scaled(
        jnp.dot(query_group, query_up, preferred_element_type=jnp.float32).reshape(
            group_rows, head_count, QK_DIM
        ),
        query_norm_gain,
    )
    queries = jnp.concatenate(
        [query_heads[..., :NOPE_DIM], rotate(query_heads[..., NOPE_DIM:], positions)], axis=-1
    ).astype(jnp.bfloat16)
    send_latent = jnp.concatenate([latent_group, context_latent], axis=0)
    send_rope = jnp.concatenate([rope_group, context_rope], axis=0)
    shard_rows = send_latent.shape[0]
    initial = (
        jnp.full((head_count, group_rows), -jnp.inf, jnp.float32),
        jnp.zeros((head_count, group_rows), jnp.float32),
        jnp.zeros((group_rows, head_count, VALUE_DIM), jnp.float32),
    )

    def latent_step(carried, parts, first_index):
        key_rows, value_rows = build_keys(
            parts[0], parts[1], first_index, shard_rows, group_rows, key_up, value_up, key_norm_gain
        )
        offset = key_offset(first_index, parts[0].shape[0], shard_rows, group_rows, context_lift)
        return attend_block(carried, queries, key_rows, value_rows, offset)

    result = fold_blocks(
        initial,
        (
            lax.all_gather(send_latent, "sp", axis=0, tiled=True),
            lax.all_gather(send_rope, "sp", axis=0, tiled=True),
        ),
        shard_rows,
        latent_step,
    )
    running_max, weight_sum, accumulated = result
    attended = (
        (accumulated / weight_sum.T[:, :, None])
        .reshape(group_rows, head_count * VALUE_DIM)
        .astype(jnp.bfloat16)
    )
    mixed_sum = lax.psum_scatter(
        jnp.dot(attended, out_weight, preferred_element_type=jnp.float32).astype(jnp.bfloat16),
        "tp",
        scatter_dimension=0,
        tiled=True,
    ).astype(jnp.float32)
    return (token_values + mod_gate * mixed_sum).astype(jnp.bfloat16)


def solution(mesh):
    in_specs = (
        P(("dp", "sp", "tp"), None),
        P(("dp", "sp")),
        P("sp", "tp"),
        P("sp", "tp"),
        P("sp", "tp"),
        P(),
        P(),
        P(),
        P(),
        P(),
        P(),
        P(None, "tp"),
        P(None, "tp"),
        P(None, "tp"),
        P(),
        P(),
        P("tp", None),
        P(("dp", "sp"), None),
        P(("dp", "sp"), None),
        P("tp"),
    )
    out_specs = P(("dp", "sp", "tp"), None)
    return jax.shard_map(local, mesh=mesh, in_specs=in_specs, out_specs=out_specs, check_vma=False)
```

profile of v0, /device:TPU:8, one launch (start us, length us, event | category | flops | bytes accessed | tf_op | source)
XLA Modules:
  0.0 202.3 jit_solution(5876710164665729727)
XLA Ops:
  11.1 9.7 %all-reduce = (f32[512]{0:T(512)S(1)}, f32[512]{0:T(512)S(1)}, f32[512]{0:T(512)}) all-reduce(f32[512]{0:T(512)S(1)} %bitcast.124, f32[512]{0:T(512)S(1)} %bitcast.123, f32[512]{0:T(512)S(1)} %bitcast.122), channel_id=1, replica_groups=mesh['sp'=4,'tp'=4,'dp'=2] {'sp'}, use_global_device_ids=true, to_apply=%region_3.4 | all-reduce | flops 1536 | bytes 12288 | tf_op jit(solution)/shard_map/psum | solution.py:144
  20.8 8.1 %all-gather.1 = f32[4,1,512]{2,1,0:T(1,128)S(1)} all-gather(f32[1,1,512]{2,1,0:T(1,128)S(1)} %bitcast.133), channel_id=1, replica_groups=mesh['sp'=4,'tp'=4,'dp'=2] {'tp'}, dimensions={0}, use_global_device_ids=true | all-gather | bytes 10240 | tf_op jit(solution)/shard_map/all_gather | solution.py:147
  28.9 8.1 %all-gather.2 = f32[4,1,512]{2,1,0:T(1,128)S(1)} all-gather(f32[1,1,512]{2,1,0:T(1,128)S(1)} %bitcast.132), channel_id=1, replica_groups=mesh['sp'=4,'tp'=4,'dp'=2] {'tp'}, dimensions={0}, use_global_device_ids=true | all-gather | bytes 10240 | tf_op jit(solution)/shard_map/all_gather | solution.py:146
  38.2 1.7 multiply_reduce_fusion.3
  40.0 8.0 %all_gather.27 = bf16[512,256]{1,0:T(8,128)(2,1)S(1)} all-gather(bf16[128,256]{1,0:T(8,128)(2,1)S(1)} %multiply_convert_fusion.1), channel_id=1, replica_groups=mesh['sp'=4,'tp'=4,'dp'=2] {'tp'}, dimensions={0}, use_global_device_ids=true | all-gather | bytes 327680 | tf_op jit(solution)/shard_map/all_gather | solution.py:163
  49.6 10.6 %all_gather.31 = bf16[512,512]{1,0:T(8,128)(2,1)S(1)} all-gather(bf16[128,512]{1,0:T(8,128)(2,1)S(1)} %multiply_convert_fusion), channel_id=1, replica_groups=mesh['sp'=4,'tp'=4,'dp'=2] {'tp'}, dimensions={0}, use_global_device_ids=true | all-gather | bytes 655360 | tf_op jit(solution)/shard_map/all_gather | solution.py:162
  63.1 6.6 %all_gather.29 = bf16[512,32]{0,1:T(8,128)(2,1)S(1)} all-gather(bf16[128,32]{0,1:T(8,128)(2,1)S(1)} %convolution_convert_fusion.2), channel_id=1, replica_groups=mesh['sp'=4,'tp'=4,'dp'=2] {'tp'}, dimensions={0}, use_global_device_ids=true | all-gather | bytes 40960 | tf_op jit(solution)/shard_map/all_gather | solution.py:164
  70.5 15.2 %all_gather.30 = bf16[3072,32]{0,1:T(8,128)(2,1)S(1)} all-gather(bf16[768,32]{0,1:T(8,128)(2,1)S(1)} %pad_maximum_fusion.6), channel_id=1, replica_groups=mesh['sp'=4,'tp'=4,'dp'=2] {'sp'}, dimensions={0}, use_global_device_ids=true | all-gather | bytes 245760 | tf_op jit(solution)/shard_map/all_gather | solution.py:198
  89.4 64.2 %while.18 = (s32[]{:T(128)}, f32[4,512]{1,0:T(4,128)S(1)}, f32[4,512]{1,0:T(4,128)S(1)}, f32[512,4,64]{0,2,1:T(8,128)S(1)}, bf16[4,768,256]{2,1,0:T(8,128)(2,1)}...) while((s32[]{:T(128)}, f32[4,512]{1,0:T(4,128)S(1)}, ...), condition=%wide.region_11.12_spmd.clone, body=%wide.region_7.11_spmd.clone.sunk | while | flops 726175488 | bytes 56559976 | solution.py:114
  94.7 3.3 %bitcast_reduce_fusion.2 = (f32[4,512]{1,0:T(4,128)S(1)}, f32[4,768,512]{2,1,0:T(8,128)}) fusion(f32[4,768]{1,0:T(4,128)S(1)} %broadcast_select_fusion.2, bf16[512,4,96]{0,2,1:T(8,128)(2,1)S(1)} %get-tuple-element.462, bf16[768,4,32]{0,2,1:T(8,128)(2,1)S(1)} %fusion.111, bf16[768,4,64]{0,2,1:T(8,128)(2,1)S(1)} %slice.81), kind=kOutput, calls=%fused_computation.1.clone.1 | convolution fusion | flops 307886080 | bytes 7294976 | tf_op jit(solution)/shard_map/while/body/eval_jaxpr/qhd,khd->hqk/dot_general | solution.py:83
  99.4 4.1 %fusion.115 = f32[512,4,64]{0,2,1:T(8,128)S(1)} fusion(bf16[768,4,64]{0,2,1:T(8,128)(2,1)S(1)} %bitcast.109, f32[4,768,512]{2,1,0:T(8,128)} %get-tuple-element.423, f32[4,512]{1,0:T(4,128)S(1)} %get-tuple-element.454, f32[4,768]{1,0:T(4,128)S(1)} %broadcast_select_fusion.2, f32[512,4,64]{0,2,1:T(8,128)S(1)} %get-tuple-element.442, ...), kind=kOutput, calls=%fused_computation.9.clone.1 | convolution fusion | flops 208011264 | bytes 7761921 | tf_op jit(solution)/shard_map/while/body/eval_jaxpr/hqk,khd->qhd/dot_general | solution.py:91
  104.0 1.4 fusion.113
  110.7 3.3 %bitcast_reduce_fusion.2 = (f32[4,512]{1,0:T(4,128)S(1)}, f32[4,768,512]{2,1,0:T(8,128)}) fusion(f32[4,768]{1,0:T(4,128)S(1)} %broadcast_select_fusion.2, bf16[512,4,96]{0,2,1:T(8,128)(2,1)S(1)} %get-tuple-element.462, bf16[768,4,32]{0,2,1:T(8,128)(2,1)S(1)} %fusion.111, bf16[768,4,64]{0,2,1:T(8,128)(2,1)S(1)} %slice.81), kind=kOutput, calls=%fused_computation.1.clone.1 | convolution fusion | flops 307886080 | bytes 7294976 | tf_op jit(solution)/shard_map/while/body/eval_jaxpr/qhd,khd->hqk/dot_general | solution.py:83
  115.4 4.1 %fusion.115 = f32[512,4,64]{0,2,1:T(8,128)S(1)} fusion(bf16[768,4,64]{0,2,1:T(8,128)(2,1)S(1)} %bitcast.109, f32[4,768,512]{2,1,0:T(8,128)} %get-tuple-element.423, f32[4,512]{1,0:T(4,128)S(1)} %get-tuple-element.454, f32[4,768]{1,0:T(4,128)S(1)} %broadcast_select_fusion.2, f32[512,4,64]{0,2,1:T(8,128)S(1)} %get-tuple-element.442, ...), kind=kOutput, calls=%fused_computation.9.clone.1 | convolution fusion | flops 208011264 | bytes 7761921 | tf_op jit(solution)/shard_map/while/body/eval_jaxpr/hqk,khd->qhd/dot_general | solution.py:91
  120.0 1.4 fusion.113
  126.8 3.3 %bitcast_reduce_fusion.2 = (f32[4,512]{1,0:T(4,128)S(1)}, f32[4,768,512]{2,1,0:T(8,128)}) fusion(f32[4,768]{1,0:T(4,128)S(1)} %broadcast_select_fusion.2, bf16[512,4,96]{0,2,1:T(8,128)(2,1)S(1)} %get-tuple-element.462, bf16[768,4,32]{0,2,1:T(8,128)(2,1)S(1)} %fusion.111, bf16[768,4,64]{0,2,1:T(8,128)(2,1)S(1)} %slice.81), kind=kOutput, calls=%fused_computation.1.clone.1 | convolution fusion | flops 307886080 | bytes 7294976 | tf_op jit(solution)/shard_map/while/body/eval_jaxpr/qhd,khd->hqk/dot_general | solution.py:83
  131.5 4.1 %fusion.115 = f32[512,4,64]{0,2,1:T(8,128)S(1)} fusion(bf16[768,4,64]{0,2,1:T(8,128)(2,1)S(1)} %bitcast.109, f32[4,768,512]{2,1,0:T(8,128)} %get-tuple-element.423, f32[4,512]{1,0:T(4,128)S(1)} %get-tuple-element.454, f32[4,768]{1,0:T(4,128)S(1)} %broadcast_select_fusion.2, f32[512,4,64]{0,2,1:T(8,128)S(1)} %get-tuple-element.442, ...), kind=kOutput, calls=%fused_computation.9.clone.1 | convolution fusion | flops 208011264 | bytes 7761921 | tf_op jit(solution)/shard_map/while/body/eval_jaxpr/hqk,khd->qhd/dot_general | solution.py:91
  136.1 1.4 fusion.113
  142.8 3.3 %bitcast_reduce_fusion.2 = (f32[4,512]{1,0:T(4,128)S(1)}, f32[4,768,512]{2,1,0:T(8,128)}) fusion(f32[4,768]{1,0:T(4,128)S(1)} %broadcast_select_fusion.2, bf16[512,4,96]{0,2,1:T(8,128)(2,1)S(1)} %get-tuple-element.462, bf16[768,4,32]{0,2,1:T(8,128)(2,1)S(1)} %fusion.111, bf16[768,4,64]{0,2,1:T(8,128)(2,1)S(1)} %slice.81), kind=kOutput, calls=%fused_computation.1.clone.1 | convolution fusion | flops 307886080 | bytes 7294976 | tf_op jit(solution)/shard_map/while/body/eval_jaxpr/qhd,khd->hqk/dot_general | solution.py:83
  147.5 4.1 %fusion.115 = f32[512,4,64]{0,2,1:T(8,128)S(1)} fusion(bf16[768,4,64]{0,2,1:T(8,128)(2,1)S(1)} %bitcast.109, f32[4,768,512]{2,1,0:T(8,128)} %get-tuple-element.423, f32[4,512]{1,0:T(4,128)S(1)} %get-tuple-element.454, f32[4,768]{1,0:T(4,128)S(1)} %broadcast_select_fusion.2, f32[512,4,64]{0,2,1:T(8,128)S(1)} %get-tuple-element.442, ...), kind=kOutput, calls=%fused_computation.9.clone.1 | convolution fusion | flops 208011264 | bytes 7761921 | tf_op jit(solution)/shard_map/while/body/eval_jaxpr/hqk,khd->qhd/dot_general | solution.py:91
  153.6 3.3 %convolution_convert_fusion.1 = bf16[512,2048]{1,0:T(8,128)(2,1)} fusion(bf16[512,256]{0,1:T(8,128)(2,1)S(1)} %bitcast.115, bf16[256,2048]{1,0:T(8,128)(2,1)} %param.38), kind=kOutput, calls=%fused_computation.70 | convolution fusion | flops 537919488 | bytes 3407872 | tf_op jit(solution)/shard_map/dot_general | solution.py:210
  157.6 8.5 %all-gather = f32[4,1,512]{2,1,0:T(1,128)S(1)} all-gather(f32[1,1,512]{2,1,0:T(1,128)S(1)} %bitcast.131), channel_id=1, replica_groups=mesh['sp'=4,'tp'=4,'dp'=2] {'tp'}, dimensions={0}, use_global_device_ids=true | all-gather | bytes 10240 | tf_op jit(solution)/shard_map/all_gather | solution.py:148
  166.1 27.4 %reduce-scatter.2.cloned.1.call-done = bf16[128,2048]{1,0:T(8,128)(2,1)} async-done(((bf16[512,2048]{1,0:T(8,128)(2,1)}), bf16[128,2048]{1,0:T(8,128)(2,1)}) %reduce-scatter.2.cloned.1.call-update) | async-done | bytes 524304 | tf_op jit(solution)/shard_map/reduce_scatter | solution.py:209
  193.5 2.0 fusion.47
  (190 shorter events, 44.8 us)
Async XLA Ops:
  6.5 42.4 %copy-start = (bf16[2048,512]{1,0:T(8,128)(2,1)S(1)}, bf16[2048,512]{1,0:T(8,128)(2,1)}, u32[]{:S(2)}) copy-start(bf16[2048,512]{1,0:T(8,128)(2,1)} %param.28) | copy-start | bytes 6291460
  6.5 31.7 %copy-start.3 = (bf16[128,2048]{1,0:T(8,128)(2,1)S(1)}, bf16[128,2048]{1,0:T(8,128)(2,1)}, u32[]{:S(2)}) copy-start(bf16[128,2048]{1,0:T(8,128)(2,1)} %param.22) | copy-start | bytes 1572868
  6.5 31.7 %copy-start.15 = (f32[2048]{0:T(1024)S(1)}, f32[2048]{0:T(1024)}, u32[]{:S(2)}) copy-start(f32[2048]{0:T(1024)} %param.27) | copy-start | bytes 24580
  6.5 82.9 %all-gather.5.cloned.1.call-start = ((), (), s32[]{:S(2)}) async-start(), calls=%async_computation.1 | async-start | bytes 1966080 | tf_op jit(solution)/shard_map/all_gather | solution.py:197
  8.6 31.3 %copy-start.13 = (f32[256]{0:T(256)S(1)}, f32[256]{0:T(256)}, u32[]{:S(2)}) copy-start(f32[256]{0:T(256)} %param.31) | copy-start | bytes 3076
  9.8 38.2 %copy-start.6 = (bf16[256,256]{1,0:T(8,128)(2,1)S(1)}, bf16[256,256]{1,0:T(8,128)(2,1)}, u32[]{:S(2)}) copy-start(bf16[256,256]{1,0:T(8,128)(2,1)} %param.39) | copy-start | bytes 393220
  28.9 20.0 %copy-start.10 = (f32[4,1,512]{2,1,0:T(1,128)}, f32[4,1,512]{2,1,0:T(1,128)S(1)}, u32[]{:S(2)}) copy-start(f32[4,1,512]{2,1,0:T(1,128)S(1)} %broadcast_add_fusion) | copy-start | bytes 24580
  36.9 12.0 %copy-start.9 = (f32[4,1,512]{2,1,0:T(1,128)}, f32[4,1,512]{2,1,0:T(1,128)S(1)}, u32[]{:S(2)}) copy-start(f32[4,1,512]{2,1,0:T(1,128)S(1)} %all-gather.2) | copy-start | bytes 24580
  38.2 11.3 %copy-start.17 = (f32[128]{0:T(128)}, f32[128]{0:T(128)S(1)}, u32[]{:S(2)}) copy-start(f32[128]{0:T(128)S(1)} %add_rsqrt_fusion.4) | copy-start | bytes 1540
  48.8 144.6 %reduce-scatter.2.cloned.1.call-start = ((), (), s32[]{:S(2)}) async-start(), calls=%async_computation.2 | async-start | bytes 2621440 | tf_op jit(solution)/shard_map/reduce_scatter | solution.py:209
  48.9 11.3 %copy-start.5 = (bf16[512,384]{1,0:T(8,128)(2,1)S(1)}, bf16[512,384]{1,0:T(8,128)(2,1)}, u32[]{:S(2)}) copy-start(bf16[512,384]{1,0:T(8,128)(2,1)} %param.33) | copy-start | bytes 1179652
  49.5 11.3 %copy-start.14 = (f32[96]{0:T(128)S(1)}, f32[96]{0:T(128)}, u32[]{:S(2)}) copy-start(f32[96]{0:T(128)} %param.36) | copy-start | bytes 1156
  61.7 27.7 %copy-start.2 = (bf16[256,256]{1,0:T(8,128)(2,1)S(1)}, bf16[256,256]{1,0:T(8,128)(2,1)}, u32[]{:S(2)}) copy-start(bf16[256,256]{1,0:T(8,128)(2,1)} %param.35) | copy-start | bytes 393220
  91.9 2.7 %copy-start.7 = (f32[4]{0:T(128)S(1)}, f32[4]{0:T(128)}, u32[]{:S(2)}) copy-start(f32[4]{0:T(128)} %get-tuple-element.463) | copy-start | bytes 52 | tf_op jit(solution)/shard_map/while
  99.4 4.6 %copy-start.1 = (f32[4,768,512]{2,1,0:T(8,128)S(1)}, f32[4,768,512]{2,1,0:T(8,128)}, u32[]{:S(2)}) copy-start(f32[4,768,512]{2,1,0:T(8,128)} %get-tuple-element.423) | copy-start | bytes 18874372 | tf_op jit(solution)/shard_map/while
  108.0 2.7 %copy-start.7 = (f32[4]{0:T(128)S(1)}, f32[4]{0:T(128)}, u32[]{:S(2)}) copy-start(f32[4]{0:T(128)} %get-tuple-element.463) | copy-start | bytes 52 | tf_op jit(solution)/shard_map/while
  115.4 4.6 %copy-start.1 = (f32[4,768,512]{2,1,0:T(8,128)S(1)}, f32[4,768,512]{2,1,0:T(8,128)}, u32[]{:S(2)}) copy-start(f32[4,768,512]{2,1,0:T(8,128)} %get-tuple-element.423) | copy-start | bytes 18874372 | tf_op jit(solution)/shard_map/while
  121.5 2.3 %copy-start.8 = (f32[96]{0:T(128)S(1)}, f32[96]{0:T(128)}, u32[]{:S(2)}) copy-start(f32[96]{0:T(128)} %get-tuple-element.460) | copy-start | bytes 1156 | tf_op jit(solution)/shard_map/while
  124.0 2.7 %copy-start.7 = (f32[4]{0:T(128)S(1)}, f32[4]{0:T(128)}, u32[]{:S(2)}) copy-start(f32[4]{0:T(128)} %get-tuple-element.463) | copy-start | bytes 52 | tf_op jit(solution)/shard_map/while
  131.4 4.6 %copy-start.1 = (f32[4,768,512]{2,1,0:T(8,128)S(1)}, f32[4,768,512]{2,1,0:T(8,128)}, u32[]{:S(2)}) copy-start(f32[4,768,512]{2,1,0:T(8,128)} %get-tuple-element.423) | copy-start | bytes 18874372 | tf_op jit(solution)/shard_map/while
  137.5 2.3 %copy-start.8 = (f32[96]{0:T(128)S(1)}, f32[96]{0:T(128)}, u32[]{:S(2)}) copy-start(f32[96]{0:T(128)} %get-tuple-element.460) | copy-start | bytes 1156 | tf_op jit(solution)/shard_map/while
  140.1 2.7 %copy-start.7 = (f32[4]{0:T(128)S(1)}, f32[4]{0:T(128)}, u32[]{:S(2)}) copy-start(f32[4]{0:T(128)} %get-tuple-element.463) | copy-start | bytes 52 | tf_op jit(solution)/shard_map/while
  147.5 4.6 %copy-start.1 = (f32[4,768,512]{2,1,0:T(8,128)S(1)}, f32[4,768,512]{2,1,0:T(8,128)}, u32[]{:S(2)}) copy-start(f32[4,768,512]{2,1,0:T(8,128)} %get-tuple-element.423) | copy-start | bytes 18874372 | tf_op jit(solution)/shard_map/while
  156.9 36.5 %copy-start.4 = (bf16[128,2048]{1,0:T(8,128)(2,1)S(1)}, bf16[128,2048]{1,0:T(8,128)(2,1)}, u32[]{:S(2)}) copy-start(bf16[128,2048]{1,0:T(8,128)(2,1)} %param.22) | copy-start | bytes 1572868
  (8 other events, 8.6 us)
Sparse Core Ops, SparseCore 0:
  49.0 40.3 all-gather.4
  157.1 36.3 reduce-scatter.1
where the time goes:
time: 205 us; the launch traced here: 202 us
  blocking collectives  74.8 us (36%)
  matrix products  51.3 us (25%)
  waiting for transfers between devices  27.5 us (13%)
  other arithmetic  25.4 us (12%)
  between operations  13.7 us (7%)
  local copies, waits for them, and re-layouts  8.85 us (4%)
    reduce_scatter x1, waiting for transfers between devices, local(): lax.psum_scatter(jnp.dot(attended, out_weight, preferred_element_type=jnp...  27.4 us
    dot_general x4, matrix products, attend_block(): jnp.einsum('hqk,khd->qhd', weights.astype(jnp.bfloat16), value_heads, pre...  16.5 us
    all_gather x1, blocking collectives, local(): lax.all_gather(send_rope, 'sp', axis=0, tiled=True)  15.2 us
    dot_general x4, matrix products, attend_block(): jnp.einsum('qhd,khd->hqk', queries, key_heads, preferred_element_type=jnp...  13.3 us
    all_gather x1, blocking collectives, local(): lax.all_gather(query_latent, 'tp', axis=0, tiled=True)  10.6 us
    psum x1, blocking collectives, local(): lax.psum((shift_term, scale_term, gate_term), 'sp')  9.66 us
    all_gather x1, blocking collectives, local(): lax.all_gather(gate_sum, 'tp', axis=0, tiled=True)  8.51 us
    all_gather x1, blocking collectives, local(): lax.all_gather(scale_sum, 'tp', axis=0, tiled=True)  8.08 us
  transfers between devices with their start and end apart: 2, of which 2 were waited for; matrix products, arithmetic and copies ran while one was open for 4% of the time, Pallas kernels for 0%

commit v1 on v0

v1 whole, which is shorter than its diff:
```python
import functools
import math

import jax
import jax.numpy as jnp
import numpy as np
from jax import lax
from jax.experimental import pallas as pl
from jax.experimental.pallas import tpu as pltpu
from jax.sharding import PartitionSpec as P

NOPE_DIM = 64
ROPE_DIM = 32
VALUE_DIM = 64
QK_DIM = 96
PAD_DIM = 128
GRID_W = 64

EPS = 1e-06
THETA = 10000.0

F32 = jnp.float32
BF16 = jnp.bfloat16


def rms_scaled(values, gain_vector):
    mean_square = jnp.mean(values * values, axis=-1, keepdims=True)
    return values * lax.rsqrt(mean_square + EPS) * gain_vector


def turn_tables(token_count):
    freq_count = ROPE_DIM // 4
    inverse = (THETA ** (-4.0 * np.arange(freq_count) / ROPE_DIM)).astype(np.float32)
    index = np.arange(token_count)
    row = (index // GRID_W).astype(np.float32)
    col = (index % GRID_W).astype(np.float32)
    angles = np.concatenate([inverse[:, None] * row, inverse[:, None] * col], axis=0)
    angles = angles.astype(np.float64)
    return np.cos(angles).astype(np.float32), np.sin(angles).astype(np.float32)


def turn(part, cosine, sine):
    f = ROPE_DIM // 4
    u0, w0, u1, w1 = part[:f], part[f : 2 * f], part[2 * f : 3 * f], part[3 * f :]
    c0, c1, s0, s1 = cosine[:f], cosine[f:], sine[:f], sine[f:]
    return jnp.concatenate(
        [u0 * c0 - w0 * s0, w0 * c0 + u0 * s0, u1 * c1 - w1 * s1, w1 * c1 + u1 * s1], axis=0
    )


def contract(a, b, dims):
    return lax.dot_general(a, b, (dims, ((), ())), preferred_element_type=F32)


def attention_kernel(
    query_ref,
    latent_ref,
    context_ref,
    query_up_ref,
    key_up_ref,
    value_up_ref,
    query_gain_ref,
    key_gain_ref,
    lift_ref,
    cos_query_ref,
    sin_query_ref,
    cos_key_ref,
    sin_key_ref,
    out_ref,
    keys,
    values,
    queries,
    scores,
    *,
    head_count,
    chunk,
    row_block,
):
    rank = key_up_ref.shape[0]
    latent_count = latent_ref.shape[0]
    context_count = context_ref.shape[0]
    key_count = latent_count + context_count
    row_count = query_ref.shape[0]
    key_gain = key_gain_ref[...]
    query_gain = query_gain_ref[...]
    eye = (
        lax.broadcasted_iota(jnp.int32, (ROPE_DIM, ROPE_DIM), 0)
        == lax.broadcasted_iota(jnp.int32, (ROPE_DIM, ROPE_DIM), 1)
    ).astype(BF16)

    def build(rows, target, width, tables, is_context):
        latent = rows[:, :rank]
        nope = contract(key_up_ref[...], latent, ((0,), (1,)))
        rope = contract(eye, rows[:, rank : rank + ROPE_DIM], ((1,), (1,)))
        rope_square = jnp.sum(rope * rope, axis=0, keepdims=True)
        rope = rope * key_gain[NOPE_DIM:]
        if tables is not None:
            rope = turn(rope, *tables)
        for head in range(head_count):
            part = nope[head * NOPE_DIM : (head + 1) * NOPE_DIM]
            square = jnp.sum(part * part, axis=0, keepdims=True) + rope_square
            inverse = lax.rsqrt(square * (1.0 / QK_DIM) + EPS)
            if is_context:
                lift = jnp.full((16, width), lift_ref[0, head] * math.sqrt(QK_DIM), F32)
                high = lift.astype(BF16).astype(F32)
                middle = (lift - high).astype(BF16).astype(F32)
                low = lift - high - middle
                index = lax.broadcasted_iota(jnp.int32, (16, width), 0)
                extra = jnp.where(
                    index == 0,
                    high,
                    jnp.where(index == 1, middle, jnp.where(index == 2, low, 0.0)),
                )
            else:
                extra = jnp.zeros((16, width), F32)
            keys[head, :, target] = jnp.concatenate(
                [
                    part * key_gain[:NOPE_DIM] * inverse,
                    rope * inverse,
                    extra,
                    jnp.zeros((16, width), F32),
                ],
                axis=0,
            ).astype(BF16)
        value = jnp.dot(latent, value_up_ref[...], preferred_element_type=F32)
        lane = lax.broadcasted_iota(jnp.int32, (width, PAD_DIM), 1)
        for pair in range(head_count // 2):
            both = value[:, pair * PAD_DIM : (pair + 1) * PAD_DIM]
            one_even = (lane == VALUE_DIM).astype(F32)
            one_odd = (lane == 0).astype(F32)
            values[2 * pair, target, :] = jnp.where(lane < VALUE_DIM, both, one_even).astype(BF16)
            values[2 * pair + 1, target, :] = jnp.where(
                lane >= VALUE_DIM, both, one_odd
            ).astype(BF16)

    def latent_chunk(i, carry):
        at = pl.ds(pl.multiple_of(i * chunk, chunk), chunk)
        build(latent_ref[at, :], at, chunk, (cos_key_ref[:, at], sin_key_ref[:, at]), False)
        return carry

    lax.fori_loop(0, latent_count // chunk, latent_chunk, 0)

    def context_chunk(i, carry):
        source = pl.ds(pl.multiple_of(i * chunk, chunk), chunk)
        target = pl.ds(pl.multiple_of(latent_count + i * chunk, chunk), chunk)
        build(context_ref[source, :], target, chunk, None, True)
        return carry

    lax.fori_loop(0, context_count // chunk, context_chunk, 0)

    projected = contract(query_up_ref[...], query_ref[...], ((0,), (1,)))
    for head in range(head_count):
        part = projected[head * QK_DIM : (head + 1) * QK_DIM]
        inverse = lax.rsqrt(jnp.mean(part * part, axis=0, keepdims=True) + EPS)
        part = part * inverse * query_gain
        turned = turn(part[NOPE_DIM:], cos_query_ref[...], sin_query_ref[...])
        extra = (
            lax.broadcasted_iota(jnp.int32, (PAD_DIM - QK_DIM, row_count), 0) < 3
        ).astype(F32)
        whole = jnp.concatenate([part[:NOPE_DIM], turned, extra], axis=0)
        queries[head] = whole.T.astype(BF16)

    scale = QK_DIM**-0.5 * math.log2(math.e)
    chunks = key_count // chunk
    blocks = row_count // row_block

    def score_chunk(slot, head, rows, index, top):
        at = slice(index * chunk, (index + 1) * chunk)
        part = jnp.dot(queries[head, rows, :], keys[head, :, at], preferred_element_type=F32)
        scores[slot, :, at] = part
        for start in range(0, chunk, PAD_DIM):
            piece = part[:, start : start + PAD_DIM]
            top = piece if top is None else jnp.maximum(top, piece)
        return top

    def weigh_chunk(slot, head, index, top, total):
        at = slice(index * chunk, (index + 1) * chunk)
        weights = jnp.exp2((scores[slot, :, at] - top) * scale).astype(BF16)
        product = jnp.dot(weights, values[head, at, :], preferred_element_type=F32)
        return product if total is None else total + product

    def both_steps(slot, head, top, next_head, next_rows):
        top = jnp.max(top, axis=1, keepdims=True)
        next_top = None
        total = None
        for index in range(chunks):
            next_top = score_chunk(1 - slot, next_head, next_rows, index, next_top)
            total = weigh_chunk(slot, head, index, top, total)
        return total, next_top

    first = None
    for index in range(chunks):
        first = score_chunk(0, 0, slice(0, row_block), index, first)

    lane = lax.broadcasted_iota(jnp.int32, (row_block, PAD_DIM), 1)

    def pair_step(pair, top):
        even, odd = 2 * pair, 2 * pair + 1
        following = jnp.minimum(even + 2, head_count - 2)
        for block in range(blocks):
            rows = slice(block * row_block, (block + 1) * row_block)
            even_total, top = both_steps(0, even, top, odd, rows)
            if block + 1 < blocks:
                next_head = even
                next_rows = slice((block + 1) * row_block, (block + 2) * row_block)
            else:
                next_head = following
                next_rows = slice(0, row_block)
            odd_total, top = both_steps(1, odd, top, next_head, next_rows)
            joined = jnp.where(
                lane < VALUE_DIM,
                even_total / even_total[:, VALUE_DIM : VALUE_DIM + 1],
                odd_total / odd_total[:, 0:1],
            )
            out_ref[rows, pl.ds(pl.multiple_of(pair * PAD_DIM, PAD_DIM), PAD_DIM)] = joined.astype(
                BF16
            )
        return top

    lax.fori_loop(0, head_count // 2, pair_step, first)


def attend(query, latent, context, query_up, key_up, value_up, gains, lift, tables):
    row_count = query.shape[0]
    key_count = latent.shape[0] + context.shape[0]
    head_count = query_up.shape[1] // QK_DIM
    row_block = min(256, row_count)
    vmem = pl.BlockSpec(memory_space=pltpu.VMEM)
    return pl.pallas_call(
        functools.partial(
            attention_kernel, head_count=head_count, chunk=512, row_block=row_block
        ),
        out_shape=jax.ShapeDtypeStruct((row_count, head_count * VALUE_DIM), BF16),
        in_specs=[vmem] * 8 + [pl.BlockSpec(memory_space=pltpu.SMEM)] + [vmem] * 4,
        out_specs=vmem,
        scratch_shapes=[
            pltpu.VMEM((head_count, PAD_DIM, key_count), BF16),
            pltpu.VMEM((head_count, key_count, PAD_DIM), BF16),
            pltpu.VMEM((head_count, row_count, PAD_DIM), BF16),
            pltpu.VMEM((2, row_block, key_count), F32),
        ],
        compiler_params=pltpu.CompilerParams(vmem_limit_bytes=60 * 1024 * 1024),
        name="attend",
    )(query, latent, context, query_up, key_up, value_up, *gains, lift, *tables)


def project_kernel(attended_ref, weight_ref, token_ref, gate_ref, out_ref):
    groups = weight_ref.shape[0]
    mixed = None
    for group in range(groups):
        term = jnp.dot(attended_ref[group], weight_ref[group], preferred_element_type=F32)
        term = term.astype(BF16).astype(F32)
        mixed = term if mixed is None else mixed + term
    out_ref[...] = (token_ref[...].astype(F32) + gate_ref[...] * mixed).astype(BF16)


def project(attended, weight, tokens, gate):
    groups, rows, width = attended.shape
    model = tokens.shape[1]
    block = min(512, model)
    return pl.pallas_call(
        project_kernel,
        grid=(model // block,),
        out_shape=jax.ShapeDtypeStruct(tokens.shape, BF16),
        in_specs=[
            pl.BlockSpec((groups, rows, width), lambda i: (0, 0, 0)),
            pl.BlockSpec((groups, width, block), lambda i: (0, 0, i)),
            pl.BlockSpec((rows, block), lambda i: (0, i)),
            pl.BlockSpec((1, block), lambda i: (0, i)),
        ],
        out_specs=pl.BlockSpec((rows, block), lambda i: (0, i)),
        name="project",
    )(attended, weight, tokens, gate)


def spread(block, axes, count):
    copies = jnp.broadcast_to(block[None], (count,) + block.shape)
    return lax.all_to_all(copies, axes, 0, 0)


def local(
    n_sp,
    n_tp,
    latent_tokens,
    condition,
    shift_weight,
    scale_weight,
    gate_weight,
    norm_gain,
    query_down,
    query_gain,
    kv_down,
    kv_gain,
    rope_down,
    query_up,
    key_up,
    value_up,
    query_norm_gain,
    key_norm_gain,
    out_weight,
    context_latent,
    context_rope,
    context_lift,
):
    model = latent_tokens.shape[1]
    activated = jax.nn.silu(condition.astype(F32)).astype(BF16)[None]
    terms = jnp.concatenate(
        [
            jnp.dot(activated, weight, preferred_element_type=F32)
            for weight in (shift_weight, scale_weight, gate_weight)
        ],
        axis=0,
    )
    gathered = spread(terms, ("sp", "tp"), n_sp * n_tp)
    context = spread(
        jnp.concatenate([context_latent, context_rope], axis=1), "sp", n_sp
    ).reshape(-1, context_latent.shape[1] + context_rope.shape[1])
    all_weight = spread(out_weight, "tp", n_tp)
    summed = jnp.sum(gathered.reshape(n_sp, n_tp, 3, -1), axis=0)
    mod = jnp.transpose(summed, (1, 0, 2)).reshape(3, model)
    token_values = latent_tokens.astype(F32)
    normed = (rms_scaled(token_values, norm_gain) * (1.0 + mod[1]) + mod[0]).astype(BF16)
    key_latent = rms_scaled(
        jnp.dot(normed, kv_down, preferred_element_type=F32), kv_gain
    ).astype(BF16)
    rope_key = jnp.dot(normed, rope_down, preferred_element_type=F32).astype(BF16)
    latent = spread(
        jnp.concatenate([key_latent, rope_key], axis=1), ("sp", "tp"), n_sp * n_tp
    ).reshape(-1, context.shape[1])
    query_latent = rms_scaled(
        jnp.dot(normed, query_down, preferred_element_type=F32), query_gain
    ).astype(BF16)
    query_group = spread(query_latent, "tp", n_tp).reshape(-1, query_latent.shape[1])
    group_rows = query_group.shape[0]
    cosine, sine = (jnp.asarray(t) for t in turn_tables(latent.shape[0]))
    start = lax.axis_index("sp") * group_rows
    own = [lax.dynamic_slice_in_dim(t, start, group_rows, 1) for t in (cosine, sine)]
    attended = attend(
        query_group,
        latent,
        context,
        query_up,
        key_up,
        value_up,
        (query_norm_gain[:, None], key_norm_gain[:, None]),
        context_lift[None],
        (*own, cosine, sine),
    )
    shared = lax.all_to_all(
        attended.reshape(n_tp, group_rows // n_tp, attended.shape[1]), "tp", 0, 0
    )
    return project(shared, all_weight, latent_tokens, mod[2:3])


def solution(mesh):
    in_specs = (
        P(("dp", "sp", "tp"), None),
        P(("dp", "sp")),
        P("sp", "tp"),
        P("sp", "tp"),
        P("sp", "tp"),
        P(),
        P(),
        P(),
        P(),
        P(),
        P(),
        P(None, "tp"),
        P(None, "tp"),
        P(None, "tp"),
        P(),
        P(),
        P("tp", None),
        P(("dp", "sp"), None),
        P(("dp", "sp"), None),
        P("tp"),
    )
    out_specs = P(("dp", "sp", "tp"), None)
    body = functools.partial(local, mesh.shape["sp"], mesh.shape["tp"])
    return jax.shard_map(body, mesh=mesh, in_specs=in_specs, out_specs=out_specs, check_vma=False)
```

time: 205 us -> 167 us (0.81)
  blocking collectives: 74.8 us -> 9.83 us
  waiting for transfers between devices: 27.5 us -> 87.2 us
  matrix products: 51.3 us -> 7.37 us
  starting transfers between devices: 0.04 us -> 27.8 us
  other arithmetic: 25.4 us -> 1.32 us
  Pallas kernels: 0 us -> 18.5 us
  between operations: 13.7 us -> 0.23 us
  local copies, waits for them, and re-layouts: 8.85 us -> 13.9 us
    all_to_all x0 -> x5, waiting for transfers between devices: none -> 87.2 us  [spread(): return lax.all_to_all(copies, axes, 0, 0)]
    all_gather x7 -> x0, blocking collectives: 65.2 us -> none  [the longest x1 15.2 us: local(): lax.all_gather(send_rope, 'sp', axis=0, tiled=True)]
    dot_general x24 -> x6, matrix products: 51.3 us -> 7.37 us  [the longest x3 3.66 us: local(): jnp.dot(activated, weight, preferred_element_type=F32)]
    all_to_all x0 -> x5, starting transfers between devices: none -> 27.8 us  [spread(): return lax.all_to_all(copies, axes, 0, 0)]
    reduce_scatter x1 -> x0, waiting for transfers between devices: 27.4 us -> none  [local(): lax.psum_scatter(jnp.dot(attended, out_weight, preferred_element_type=jnp...]
    pallas_call x0 -> x2, Pallas kernels: none -> 18.5 us  [the longest x1 13.8 us: attend(): pl.pallas_call(functools.partial(attention_kernel, head_count=head_count,...]
    all_to_all x0 -> x1, blocking collectives: none -> 9.83 us  [local(): lax.all_to_all(attended.reshape(n_tp, group_rows // n_tp, attended.shape[...]
    psum x1 -> x0, blocking collectives: 9.66 us -> none  [local(): lax.psum((shift_term, scale_term, gate_term), 'sp')]
  transfers between devices with their start and end apart: 2 -> 5, of which waited for: 2 -> 5; matrix products, arithmetic and copies ran while one was open for 4% -> 7% of each run, Pallas kernels for 0% -> 0%
where the time goes in v1:
time: 167 us; the launch traced here: 166 us
  waiting for transfers between devices  87.2 us (52%)
  starting transfers between devices  27.8 us (17%)
  Pallas kernels  18.5 us (11%)
  local copies, waits for them, and re-layouts  13.9 us (8%)
  blocking collectives  9.83 us (6%)
  matrix products  7.37 us (4%)
    all_to_all x5, waiting for transfers between devices, spread(): return lax.all_to_all(copies, axes, 0, 0)  87.2 us
    all_to_all x5, starting transfers between devices, spread(): return lax.all_to_all(copies, axes, 0, 0)  27.8 us
    pallas_call x1, Pallas kernels, attend(): pl.pallas_call(functools.partial(attention_kernel, head_count=head_count,...  13.8 us
    all_to_all x1, blocking collectives, local(): lax.all_to_all(attended.reshape(n_tp, group_rows // n_tp, attended.shape[...  9.83 us
    broadcast_in_dim x5, local copies, waits for them, and re-layouts, spread(): copies = jnp.broadcast_to(block[None], (count,) + block.shape)  6.09 us
    pallas_call x1, Pallas kernels, project(): pl.pallas_call(project_kernel, grid=(model // block,), out_shape=jax.Shap...  4.72 us
    all_to_all x2, local copies, waits for them, and re-layouts, spread(): return lax.all_to_all(copies, axes, 0, 0)  3.8 us
    dot_general x3, matrix products, local(): jnp.dot(activated, weight, preferred_element_type=F32)  3.66 us
  transfers between devices with their start and end apart: 5, of which 5 were waited for; matrix products, arithmetic and copies ran while one was open for 7% of the time, Pallas kernels for 0%

profile of v1, /device:TPU:8, one launch (start us, length us, event | category | flops | bytes accessed | tf_op | source)
XLA Modules:
  0.0 166.1 jit_solution(13170134911848951289)
XLA Ops:
  0.0 0.8 fusion.8
  0.9 1.2 fusion.16
  2.1 1.2 fusion.15
  3.3 1.2 fusion.14
  5.2 7.2 %all-to-all-start = ((f32[16,3,512]{2,1,0:T(4,128)}), f32[16,3,512]{2,1,0:T(4,128)S(1)}, u32[]{:S(2)}, u32[]{:S(2)}) async-start(f32[16,3,512]{2,1,0:T(4,128)} %broadcast_in_dim.16), calls=%async_computation | async-start | bytes 262144 | tf_op jit(solution)/shard_map/all_to_all | solution.py:278
  13.0 6.1 %all-to-all-done = f32[16,3,512]{2,1,0:T(4,128)S(1)} async-done(((f32[16,3,512]{2,1,0:T(4,128)}), f32[16,3,512]{2,1,0:T(4,128)S(1)}, u32[]{:S(2)}, u32[]{:S(2)}) %all-to-all-start) | async-done | bytes 98336 | tf_op jit(solution)/shard_map/all_to_all | solution.py:278
  19.1 0.9 broadcast_in_dim.19
  19.9 4.7 %all-to-all-start.3 = ((bf16[4,256,288]{1,2,0:T(8,128)(2,1)}), bf16[4,256,288]{1,2,0:T(8,128)(2,1)S(1)}, u32[]{:S(2)}, u32[]{:S(2)}) async-start(bf16[4,256,288]{1,2,0:T(8,128)(2,1)} %broadcast_in_dim.19), calls=%async_computation.3 | async-start | bytes 1179648 | tf_op jit(solution)/shard_map/all_to_all | solution.py:278
  25.3 1.7 %multiply_reduce_fusion.1 = (f32[128]{0:T(128)S(1)}, f32[128,256]{1,0:T(8,128)S(1)}) fusion(bf16[2048,256]{1,0:T(8,128)(2,1)} %param.30, bf16[128,2048]{1,0:T(8,128)(2,1)S(1)} %copy-done.2, f32[2048]{0:T(1024)S(1)} %bitcast.39, f32[2048]{0:T(1024)S(1)} %bitcast.42, f32[2048]{0:T(1024)S(1)} %copy-done.11, f32[128]{0:T(128)S(1)} %add_rsqrt_fusion.2), kind=kOutput, calls=%fused_computation.12 | convolution fusion | flops 135856000 | bytes 1729536 | tf_op jit(solution)/shard_map/dot_general | solution.py:324
  27.3 8.9 %all-to-all-done.3 = bf16[4,256,288]{1,2,0:T(8,128)(2,1)S(1)} async-done(((bf16[4,256,288]{1,2,0:T(8,128)(2,1)}), bf16[4,256,288]{1,2,0:T(8,128)(2,1)S(1)}, u32[]{:S(2)}, u32[]{:S(2)}) %all-to-all-start.3) | async-done | bytes 589856 | tf_op jit(solution)/shard_map/all_to_all | solution.py:278
  36.1 1.2 broadcast_in_dim.18
  37.4 6.8 %all-to-all-start.2 = ((bf16[16,128,288]{1,2,0:T(8,128)(2,1)}), bf16[16,128,288]{1,2,0:T(8,128)(2,1)S(1)}, u32[]{:S(2)}, u32[]{:S(2)}) async-start(bf16[16,128,288]{1,2,0:T(8,128)(2,1)} %broadcast_in_dim.18), calls=%async_computation.2 | async-start | bytes 2359296 | tf_op jit(solution)/shard_map/all_to_all | solution.py:278
  44.2 1.6 multiply_reduce_fusion
  46.0 26.2 %all-to-all-done.2 = bf16[16,128,288]{1,2,0:T(8,128)(2,1)S(1)} async-done(((bf16[16,128,288]{1,2,0:T(8,128)(2,1)}), bf16[16,128,288]{1,2,0:T(8,128)(2,1)S(1)}, u32[]{:S(2)}, u32[]{:S(2)}) %all-to-all-start.2) | async-done | bytes 1179680 | tf_op jit(solution)/shard_map/all_to_all | solution.py:278
  73.1 4.1 %all-to-all-start.1 = ((bf16[4,128,512]{2,1,0:T(8,128)(2,1)}), bf16[4,128,512]{2,1,0:T(8,128)(2,1)}, u32[]{:S(2)}, u32[]{:S(2)}) async-start(bf16[4,128,512]{2,1,0:T(8,128)(2,1)} %broadcast_in_dim.17), calls=%async_computation.1 | async-start | bytes 1048576 | tf_op jit(solution)/shard_map/all_to_all | solution.py:278
  78.7 1.4 constant_dynamic-slice_fusion
  80.1 2.2 %copy.69 = bf16[4,256,288]{2,1,0:T(8,128)(2,1)} copy(bf16[4,256,288]{1,2,0:T(8,128)(2,1)} %copy-done.1) | data formatting | bytes 1179648 | tf_op jit(solution)/shard_map/all_to_all | solution.py:278
  82.3 1.6 copy.66
  84.4 13.8 %attend.1 = bf16[512,256]{1,0:T(8,128)(2,1)} custom-call(bf16[512,512]{1,0:T(8,128)(2,1)} %bitcast.5.query_ref, bf16[2048,288]{1,0:T(8,128)(2,1)} %bitcast.32, bf16[1024,288]{1,0:T(8,128)(2,1)} %bitcast.33, bf16[512,384]{1,0:T(8,128)(2,1)} %query_up_ref.1, bf16[256,256]{1,0:T(8,128)(2,1)} %key_up_ref.1, bf16[256,256]{1,0:T(8,128)(2,1)} %value_up_ref.1, ...), custom_call_target="tpu_custom_call" | custom-call | tf_op jit(solution)/shard_map/attend/pallas_call | solution.py:229
  98.2 9.8 %all_to_all.30.attended_ref = bf16[4,128,256]{2,1,0:T(8,128)(2,1)} all-to-all(bf16[4,128,256]{2,1,0:T(8,128)(2,1)} %bitcast.34), channel_id=1, replica_groups=mesh['sp'=4,'tp'=4,'dp'=2] {'tp'}, dimensions={0} | all-to-all | bytes 524288 | tf_op jit(solution)/shard_map/all_to_all | solution.py:349
  108.0 2.5 %broadcast_in_dim.23 = bf16[4,256,2048]{2,1,0:T(8,128)(2,1)} broadcast(bf16[256,2048]{1,0:T(8,128)(2,1)S(1)} %copy-done.3), dimensions={1,2} | broadcast | bytes 5242880 | tf_op jit(solution)/shard_map/broadcast_in_dim | solution.py:277
  110.5 4.8 %all-to-all-start.5 = ((bf16[4,256,2048]{2,1,0:T(8,128)(2,1)}), bf16[4,256,2048]{2,1,0:T(8,128)(2,1)}, u32[]{:S(2)}, u32[]{:S(2)}) async-start(bf16[4,256,2048]{2,1,0:T(8,128)(2,1)} %broadcast_in_dim.23), calls=%async_computation.5 | async-start | bytes 8388608 | tf_op jit(solution)/shard_map/all_to_all | solution.py:278
  116.0 45.4 %all-to-all-done.5.weight_ref = bf16[4,256,2048]{2,1,0:T(8,128)(2,1)} async-done(((bf16[4,256,2048]{2,1,0:T(8,128)(2,1)}), bf16[4,256,2048]{2,1,0:T(8,128)(2,1)}, u32[]{:S(2)}, u32[]{:S(2)}) %all-to-all-start.5) | async-done | bytes 4194336 | tf_op jit(solution)/shard_map/all_to_all | solution.py:278
  161.4 4.7 %project.1 = bf16[128,2048]{1,0:T(8,128)(2,1)} custom-call(bf16[4,128,256]{2,1,0:T(8,128)(2,1)} %all_to_all.30.attended_ref, bf16[4,256,2048]{2,1,0:T(8,128)(2,1)} %all-to-all-done.5.weight_ref, bf16[128,2048]{1,0:T(8,128)(2,1)} %token_ref.1, f32[1,2048]{1,0:T(1,128)} %bitcast.37), custom_call_target="tpu_custom_call" | custom-call | tf_op jit(solution)/shard_map/project/pallas_call | solution.py:261
  (50 shorter events, 5.5 us)
Async XLA Ops:
  0.0 44.2 %copy-start = (bf16[2048,512]{1,0:T(8,128)(2,1)S(1)}, bf16[2048,512]{1,0:T(8,128)(2,1)}, u32[]{:S(2)}) copy-start(bf16[2048,512]{1,0:T(8,128)(2,1)} %param.28) | copy-start | bytes 6291460
  0.0 12.5 %copy-start.2 = (bf16[128,2048]{1,0:T(8,128)(2,1)S(1)}, bf16[128,2048]{1,0:T(8,128)(2,1)}, u32[]{:S(2)}) copy-start(bf16[128,2048]{1,0:T(8,128)(2,1)} %token_ref.1) | copy-start | bytes 1572868
  0.0 12.7 %copy-start.5 = (bf16[256,32]{0,1:T(8,128)(2,1)S(1)}, bf16[256,32]{0,1:T(8,128)(2,1)}, u32[]{:S(2)}) copy-start(bf16[256,32]{0,1:T(8,128)(2,1)} %param.40) | copy-start | bytes 49156
  0.0 12.8 %copy-start.4 = (bf16[256,256]{1,0:T(8,128)(2,1)S(1)}, bf16[256,256]{1,0:T(8,128)(2,1)}, u32[]{:S(2)}) copy-start(bf16[256,256]{1,0:T(8,128)(2,1)} %param.39) | copy-start | bytes 393220
  4.5 20.2 %copy-start.10 = (bf16[2048,32]{0,1:T(8,128)(2,1)S(1)}, bf16[2048,32]{0,1:T(8,128)(2,1)}, u32[]{:S(2)}) copy-start(bf16[2048,32]{0,1:T(8,128)(2,1)} %param.32) | copy-start | bytes 393220
  4.5 20.2 %copy-start.11 = (f32[2048]{0:T(1024)S(1)}, f32[2048]{0:T(1024)}, u32[]{:S(2)}) copy-start(f32[2048]{0:T(1024)} %param.27) | copy-start | bytes 24580
  5.2 13.8 %all-to-all-start = ((f32[16,3,512]{2,1,0:T(4,128)}), f32[16,3,512]{2,1,0:T(4,128)S(1)}, u32[]{:S(2)}, u32[]{:S(2)}) async-start(f32[16,3,512]{2,1,0:T(4,128)} %broadcast_in_dim.16), calls=%async_computation | async-start | bytes 262144 | tf_op jit(solution)/shard_map/all_to_all | solution.py:278
  19.9 16.2 %all-to-all-start.3 = ((bf16[4,256,288]{1,2,0:T(8,128)(2,1)}), bf16[4,256,288]{1,2,0:T(8,128)(2,1)S(1)}, u32[]{:S(2)}, u32[]{:S(2)}) async-start(bf16[4,256,288]{1,2,0:T(8,128)(2,1)} %broadcast_in_dim.19), calls=%async_computation.3 | async-start | bytes 1179648 | tf_op jit(solution)/shard_map/all_to_all | solution.py:278
  24.7 2.3 %copy-start.7 = (f32[256]{0:T(256)S(1)}, f32[256]{0:T(256)}, u32[]{:S(2)}) copy-start(f32[256]{0:T(256)} %param.31) | copy-start | bytes 3076
  36.1 1.2 copy-start.1
  37.4 34.9 %all-to-all-start.2 = ((bf16[16,128,288]{1,2,0:T(8,128)(2,1)}), bf16[16,128,288]{1,2,0:T(8,128)(2,1)S(1)}, u32[]{:S(2)}, u32[]{:S(2)}) async-start(bf16[16,128,288]{1,2,0:T(8,128)(2,1)} %broadcast_in_dim.18), calls=%async_computation.2 | async-start | bytes 2359296 | tf_op jit(solution)/shard_map/all_to_all | solution.py:278
  44.2 1.7 %copy-start.6 = (f32[512]{0:T(512)S(1)}, f32[512]{0:T(512)}, u32[]{:S(2)}) copy-start(f32[512]{0:T(512)} %param.29) | copy-start | bytes 6148
  44.2 33.0 %copy-start.8 = (f32[96]{0:T(128)S(1)}, f32[96]{0:T(128)}, u32[]{:S(2)}) copy-start(f32[96]{0:T(128)} %param.36) | copy-start | bytes 1156
  44.2 33.7 %copy-start.9 = (f32[96]{0:T(128)S(1)}, f32[96]{0:T(128)}, u32[]{:S(2)}) copy-start(f32[96]{0:T(128)} %param.37) | copy-start | bytes 1156
  73.1 11.4 %all-to-all-start.1 = ((bf16[4,128,512]{2,1,0:T(8,128)(2,1)}), bf16[4,128,512]{2,1,0:T(8,128)(2,1)}, u32[]{:S(2)}, u32[]{:S(2)}) async-start(bf16[4,128,512]{2,1,0:T(8,128)(2,1)} %broadcast_in_dim.17), calls=%async_computation.1 | async-start | bytes 1048576 | tf_op jit(solution)/shard_map/all_to_all | solution.py:278
  84.4 23.6 %copy-start.3 = (bf16[256,2048]{1,0:T(8,128)(2,1)S(1)}, bf16[256,2048]{1,0:T(8,128)(2,1)}, u32[]{:S(2)}) copy-start(bf16[256,2048]{1,0:T(8,128)(2,1)} %param.38) | copy-start | bytes 3145732
  110.5 50.9 %all-to-all-start.5 = ((bf16[4,256,2048]{2,1,0:T(8,128)(2,1)}), bf16[4,256,2048]{2,1,0:T(8,128)(2,1)}, u32[]{:S(2)}, u32[]{:S(2)}) async-start(bf16[4,256,2048]{2,1,0:T(8,128)(2,1)} %broadcast_in_dim.23), calls=%async_computation.5 | async-start | bytes 8388608 | tf_op jit(solution)/shard_map/all_to_all | solution.py:278
